TPU v7x, 32 devices: a whole 2x2x4 slice. The times are simulated.
32 devices in a mesh: kv: 8 (over z, y), tp: 4 (over x, core).
Axes of the slice: x: 2, y: 2, z: 4, core: 2. Of those that a mesh axis runs over, the one named last changes fastest.
Arguments:
- queries: bfloat16 [1024, 1024], P('kv', 'tp'), may hold values from -6 to 6
- keys: bfloat16 [1024, 512], P('kv', 'tp'), may hold values from -6 to 6
- values: bfloat16 [1024, 512], P('kv', 'tp'), may hold values from -6 to 6
- hidden: bfloat16 [1024, 2048], P('kv'), may hold values from -6 to 6
- log_sums: float32 [2, 1024, 16], P(None, 'kv', 'tp'), may hold values from -1 to 12
- gates: float32 [2, 1024, 16], P(None, 'kv', 'tp'), may hold values from 0.1 to 0.9
- branch_out: bfloat16 [2, 1024, 1024], P(None, 'kv', 'tp'), may hold values from -6 to 6
- cotangent: bfloat16 [1024, 1024], P('kv', 'tp'), may hold values from -6 to 6
- chosen: int32 [8, 8, 48], P(None, 'tp'), may hold values from -1 to 31, as said below
Outputs:
- grad_queries: float32 [1024, 1024], P('kv', 'tp')
- grad_keys: float32 [1024, 512], P('kv', 'tp')
- grad_values: float32 [1024, 512], P('kv', 'tp')
- grad_weight: float32 [2048, 1024], P('kv', 'tp')
Inputs may be any that keep to these rules, and one draw needn't show every extreme that they name: `chosen`: each list holds global block numbers or -1. All live entries of one list name blocks of distinct owners, owner = entry // 4, none later than the list's range; list d holds min(48, d + 1) live entries, and they come first.
All inputs are finite; a program needn't handle non-finite values.
Results may differ from a plain program's by a relative error of at most 0.0055.
Values may be sent and summed in bfloat16 or wider, within the bound.
A program may use at most 64 MiB of HBM per device.

v0:
```python
import jax
import jax.numpy as jnp
from jax import lax
from jax.sharding import PartitionSpec as P

DH = 64
BLK = 32
TOPN = 12
SUB = 4
CMP = 32


def branch_grads(query_rows, key_rows, value_rows, seen, log_rows, delta_rows, cot_rows, scale):
    wide = jnp.float32
    scores = jnp.einsum("tgre,gme->grtm", query_rows, key_rows, preferred_element_type=wide) * scale
    log_here = jnp.transpose(log_rows, (1, 2, 0))[..., None]
    delta_here = jnp.transpose(delta_rows, (1, 2, 0))[..., None]
    probs = jnp.where(seen[:, None], jnp.exp(scores - log_here), 0.0)
    probs_low = probs.astype(jnp.bfloat16)
    value_grad = jnp.einsum("grtm,tgre->gme", probs_low, cot_rows, preferred_element_type=wide)
    prob_grad = jnp.einsum("tgre,gme->grtm", cot_rows, value_rows, preferred_element_type=wide)
    score_low = (probs * (prob_grad - delta_here)).astype(jnp.bfloat16)
    query_grad = (
        jnp.einsum("grtm,gme->tgre", score_low, key_rows, preferred_element_type=wide) * scale
    )
    key_grad = (
        jnp.einsum("grtm,tgre->gme", score_low, query_rows, preferred_element_type=wide) * scale
    )
    return (query_grad, key_grad, value_grad)


def shards(queries, keys, values, hidden, log_sums, gates, branch_out, cotangent, chosen):
    wide = jnp.float32
    rows_here = queries.shape[0]
    heads = queries.shape[1] // DH
    groups = keys.shape[1] // DH
    group_heads = heads // groups
    per_block = rows_here // BLK
    per_summary = rows_here // CMP
    blocks_all = chosen.shape[0]
    nsel = chosen.shape[2]
    qrows = rows_here // SUB
    scale = DH ** (-0.5)
    grads_each = jax.vmap(branch_grads, in_axes=(0, 0, 0, 0, 0, 0, 0, None))
    place = lax.axis_index("kv")
    position = place * rows_here + jnp.arange(rows_here, dtype=jnp.int32)
    gated = gates[..., None] * cotangent.reshape(rows_here, heads, DH).astype(wide)[None]
    delta_all = jnp.sum(gated * branch_out.reshape(2, rows_here, heads, DH).astype(wide), -1)
    delta_all = delta_all.reshape(2, rows_here, groups, group_heads)
    gated_low = gated.astype(jnp.bfloat16).reshape(2, rows_here, groups, group_heads, DH)
    log_all = log_sums.reshape(2, rows_here, groups, group_heads)
    query_all = queries.reshape(rows_here, groups, group_heads, DH)
    pairs = jnp.concatenate(
        [keys.reshape(rows_here, groups, DH), values.reshape(rows_here, groups, DH)], -1
    )
    means = jnp.mean(pairs.reshape(per_summary, CMP, groups, 2 * DH).astype(wide), 1).astype(
        jnp.bfloat16
    )
    summaries = lax.all_gather(means, "kv", axis=0, tiled=True)
    summary_count = summaries.shape[0]
    sum_keys = jnp.transpose(summaries[..., :DH], (1, 0, 2))
    sum_values = jnp.transpose(summaries[..., DH:], (1, 0, 2))
    summary_end = jnp.arange(summary_count, dtype=jnp.int32) * CMP + CMP - 1
    summary_seen = (summary_end[None, :] <= position[:, None])[None]
    query_sum, key_sum, value_sum = branch_grads(
        query_all, sum_keys, sum_values, summary_seen, log_all[0], delta_all[0], gated_low[0], scale
    )
    summary_term = jnp.transpose(jnp.concatenate([key_sum, value_sum], -1), (1, 0, 2))
    listing = lax.dynamic_index_in_dim(chosen, place, 0, keepdims=False)
    live = listing >= 0
    safe = jnp.maximum(listing, 0)
    owner = safe // per_block
    group_index = jnp.arange(groups, dtype=jnp.int32)
    hits = (chosen >= 0) & (chosen // per_block == place)
    wanted = jnp.sum(jnp.where(hits, chosen % per_block, 0), -1)
    asked = jnp.any(hits, -1)
    row_target = safe[..., None] * BLK + jnp.arange(BLK, dtype=jnp.int32)
    pair_blocks = pairs.reshape(per_block, BLK, groups, 2 * DH)
    outbound = pair_blocks[wanted, :, group_index[None, :], :]
    arrived = lax.all_to_all(outbound, "kv", split_axis=0, concat_axis=0, tiled=True)
    picked = arrived[owner, group_index[:, None]]

    def by_sub(array):
        rest = array.shape[3:]
        moved = array.reshape((groups, SUB, TOPN * BLK) + rest)
        return jnp.swapaxes(moved, 0, 1)

    picked_sub = by_sub(picked)
    picked_keys = picked_sub[..., :DH]
    picked_values = picked_sub[..., DH:]
    live_rows = by_sub(jnp.broadcast_to(live[..., None], (groups, nsel, BLK)))
    key_position = by_sub(row_target)
    sub_position = position.reshape(SUB, qrows)
    block_seen = live_rows[:, :, None, :] & (
        key_position[:, :, None, :] <= sub_position[:, None, :, None]
    )
    query_sel, key_sel, value_sel = grads_each(
        query_all.reshape(SUB, qrows, groups, group_heads, DH),
        picked_keys,
        picked_values,
        block_seen,
        log_all[1].reshape(SUB, qrows, groups, group_heads),
        delta_all[1].reshape(SUB, qrows, groups, group_heads),
        gated_low[1].reshape(SUB, qrows, groups, group_heads, DH),
        scale,
    )
    query_sel = query_sel.reshape(rows_here, groups, group_heads, DH)
    key_sel = jnp.swapaxes(key_sel, 0, 1).reshape(groups, nsel, BLK, DH)
    value_sel = jnp.swapaxes(value_sel, 0, 1).reshape(groups, nsel, BLK, DH)
    slot_grads = jnp.concatenate([key_sel, value_sel], -1)
    slot_grads = slot_grads * live[..., None, None].astype(wide)
    outgoing = (
        jnp.zeros((blocks_all, groups, BLK, 2 * DH), wide)
        .at[owner, group_index[:, None]]
        .add(slot_grads)
    )
    summary_out = jnp.transpose(
        summary_term.reshape(blocks_all, per_summary, groups, 2 * DH), (0, 2, 1, 3)
    )
    both_out = jnp.concatenate([outgoing, summary_out], 2)
    both_in = lax.all_to_all(
        both_out.astype(jnp.bfloat16), "kv", split_axis=0, concat_axis=0, tiled=True
    ).astype(both_out.dtype)
    incoming = both_in[:, :, :BLK]
    summary_mine = jnp.transpose(jnp.sum(both_in[:, :, BLK:], 0), (1, 0, 2))
    selector = (
        (wanted[..., None] == jnp.arange(per_block, dtype=jnp.int32)) & asked[..., None]
    ).astype(wide)
    block_sums = jnp.einsum("rgb,rgkc->bkgc", selector, incoming, precision=lax.Precision.HIGHEST)
    pair_grads = (
        block_sums.reshape(rows_here, groups, 2 * DH) + jnp.repeat(summary_mine, CMP, axis=0) / CMP
    )
    grad_queries = (query_sum + query_sel).reshape(rows_here, heads * DH)
    query_low = grad_queries.astype(jnp.bfloat16)
    grad_weight = lax.psum_scatter(
        lax.dot_general(
            hidden, query_low, (((0,), (0,)), ((), ())), preferred_element_type=jnp.float32
        ),
        "kv",
        scatter_dimension=0,
        tiled=True,
    )
    grad_keys = pair_grads[..., :DH].reshape(rows_here, groups * DH)
    grad_values = pair_grads[..., DH:].reshape(rows_here, groups * DH)
    return (grad_queries, grad_keys, grad_values, grad_weight)


def solution(mesh):
    return jax.shard_map(
        shards,
        mesh=mesh,
        in_specs=(
            P("kv", "tp"),
            P("kv", "tp"),
            P("kv", "tp"),
            P("kv", None),
            P(None, "kv", "tp"),
            P(None, "kv", "tp"),
            P(None, "kv", "tp"),
            P("kv", "tp"),
            P(None, "tp", None),
        ),
        out_specs=(P("kv", "tp"), P("kv", "tp"), P("kv", "tp"), P("kv", "tp")),
        check_vma=False,
    )
```

profile of v0, /device:TPU:0, one launch (start us, length us, event | category | flops | bytes accessed | tf_op | source)
XLA Modules:
  0.0 136.0 jit_solution(15902463175480948571)
XLA Ops:
  7.2 1.0 fusion.44
  8.2 0.9 fusion.33
  9.1 0.1 copy.157
  9.2 0.1 copy.158
  9.3 0.1 reshape.249
  9.4 0.8 concatenate.26
  10.3 0.8 concatenate.27
  11.1 0.1 convert_reduce_fusion
  11.3 1.3 gather_fusion
  12.5 7.3 %all-to-all-start = ((bf16[8,2,32,128]{3,2,1,0:T(8,128)(2,1)}), bf16[8,2,32,128]{3,2,1,0:T(8,128)(2,1)S(1)}, u32[]{:S(2)}, u32[]{:S(2)}) async-start(bf16[8,2,32,128]{3,2,1,0:T(8,128)(2,1)} %bitcast.20), calls=%async_computation | async-start | bytes 262144 | tf_op jit(solution)/shard_map/all_to_all | solution.py:80
  19.9 0.7 multiply_bitcast_fusion.1
  20.6 0.7 fusion.45
  21.3 0.7 or_select_fusion
  22.0 1.0 copy.153
  22.9 1.0 reshape_reshape.3
  23.9 0.1 reshape.255
  24.0 0.1 add.117
  24.1 0.1 broadcast_in_dim.36
  24.2 0.1 reshape.239
  24.4 0.1 add.115
  24.5 26.6 %all_gather.3 = bf16[32,2,128]{2,1,0:T(2,128)(2,1)S(1)} all-gather(bf16[4,2,128]{2,1,0:T(2,128)(2,1)S(1)} %multiply_convert_fusion.1), channel_id=1, replica_groups=mesh['kv'=8,'tp'=4] {'kv'}, dimensions={0}, use_global_device_ids=true | all-gather | bytes 18432 | tf_op jit(solution)/shard_map/all_gather | solution.py:59
  51.1 0.1 fusion.48
  51.2 0.1 copy.155
  51.4 0.1 copy.156
  51.7 0.1 compare_and_fusion
  51.8 0.1 fusion.18
  52.0 0.1 reshape_squeeze.9
  52.1 0.1 reshape_squeeze.11
  52.2 0.1 copy.164
  52.3 0.1 fusion.19
  52.4 1.2 gather_fusion.1
  53.6 0.4 copy.159
  54.0 0.3 fusion.5
  54.3 0.3 fusion.8
  54.6 0.3 fusion.9
  54.9 0.3 copy-done.1
  55.2 0.1 copy.168
  55.3 0.2 fusion.12
  55.5 1.8 %convolution_bitcast_fusion = f32[2048,256]{0,1:T(8,128)} fusion(bf16[128,2048]{1,0:T(8,128)(2,1)S(1)} %copy-done, f32[128,256]{0,1:T(8,128)S(1)} %bitcast.188), kind=kOutput, calls=%fused_computation.3 | convolution fusion | flops 134250496 | bytes 2752512 | tf_op jit(solution)/shard_map/dot_general | solution.py:136
  57.3 0.1 reshape.261
  57.4 0.1 fusion.21
  57.5 0.1 fusion.22
  57.7 0.1 pad_maximum_fusion.2
  57.8 0.4 copy-done.3
  58.2 0.3 fusion.7
  58.5 0.5 copy.170
  59.0 1.4 %convolution_bitcast_fusion.1 = f32[2,4,384,64]{2,3,0,1:T(8,128)S(1)} fusion(f32[4,2,2,32,384]{4,3,2,1,0:T(8,128)} %copy-done.1, bf16[4,32,2,2,64]{4,1,0,3,2:T(8,128)(2,1)S(1)} %bitcast.187), kind=kOutput, calls=%fused_computation.5 | convolution fusion | flops 25362432 | bytes 1638400 | tf_op jit(solution)/shard_map/vmap(grtm,tgre->gme)/dot_general | solution.py:20
  60.4 1.6 %copy.172 = f32[2,4,384,64]{3,2,1,0:T(8,128)} copy(f32[2,4,384,64]{2,3,0,1:T(8,128)S(1)} %convolution_bitcast_fusion.1) | data formatting | bytes 1572864 | tf_op jit(solution)/shard_map/transpose | solution.py:109
  62.1 3.2 %maximum_multiply_fusion = f32[2,48,32,128]{3,2,1,0:T(8,128)} fusion(f32[2,48,32,64]{3,2,1,0:T(8,128)} %bitcast.180, f32[2,48,32,64]{3,2,1,0:T(8,128)S(1)} %bitcast.178, f32[2,48]{1,0:T(2,128)S(1)} %get-tuple-element.30), kind=kLoop, calls=%fused_computation.4 | loop fusion | flops 786432 | bytes 3146112 | tf_op jit(solution)/shard_map/mul | solution.py:111
  65.3 9.7 %scatter_fusion = f32[8,2,32,128]{3,2,1,0:T(8,128)S(1)} fusion(f32[8,2,32,128]{3,2,1,0:T(8,128)S(1)} %broadcast_in_dim.39, s32[96]{0:T(128)S(1)} %reshape.261, f32[96,32,128]{2,1,0:T(8,128)} %bitcast.179), kind=kCustom, calls=%fused_computation.2 | custom fusion | flops 393216 | bytes 4719360 | tf_op jit(solution)/shard_map/scatter-add | solution.py:115
  75.1 0.8 copy.174
  75.9 3.9 %all-to-all-start.1 = ((bf16[8,2,36,128]{3,1,2,0:T(2,128)(2,1)}), bf16[8,2,36,128]{3,1,2,0:T(2,128)(2,1)S(1)}, u32[]{:S(2)}, u32[]{:S(2)}) async-start(bf16[8,2,36,128]{3,1,2,0:T(2,128)(2,1)} %copy.174), calls=%async_computation.1 | async-start | bytes 294912 | tf_op jit(solution)/shard_map/all_to_all | solution.py:121
  79.8 0.1 copy.177
  79.9 0.8 copy.182
  80.6 8.5 %all-to-all-done.1 = bf16[8,2,36,128]{3,1,2,0:T(2,128)(2,1)S(1)} async-done(((bf16[8,2,36,128]{3,1,2,0:T(2,128)(2,1)}), bf16[8,2,36,128]{3,1,2,0:T(2,128)(2,1)S(1)}, u32[]{:S(2)}, u32[]{:S(2)}) %all-to-all-start.1) | async-done | bytes 147488 | tf_op jit(solution)/shard_map/all_to_all | solution.py:121
  89.2 0.1 slice.80
  89.3 0.3 fusion.10
  89.6 0.1 fusion.46
  89.7 0.1 copy.181
  89.8 0.7 copy.184
  90.5 0.1 copy.180
  90.6 0.7 copy.183
  91.3 36.1 %reduce-scatter.2.cloned.1.call-done = f32[256,256]{0,1:T(8,128)} async-done(((f32[2048,256]{0,1:T(8,128)}), f32[256,256]{0,1:T(8,128)}) %reduce-scatter.2.cloned.1.call-update) | async-done | bytes 262160 | tf_op jit(solution)/shard_map/reduce_scatter | solution.py:135
  127.4 1.8 %copy.185 = f32[256,256]{1,0:T(8,128)} copy(f32[256,256]{0,1:T(8,128)} %reduce-scatter.2.cloned.1.call-done) | data formatting | bytes 524288
  (47 shorter events, 0.6 us)
Async XLA Ops:
  7.2 48.4 %copy-start = (bf16[128,2048]{1,0:T(8,128)(2,1)S(1)}, bf16[128,2048]{1,0:T(8,128)(2,1)}, u32[]{:S(2)}) copy-start(bf16[128,2048]{1,0:T(8,128)(2,1)} %param.12) | copy-start | bytes 1572868
  7.2 16.8 %copy-start.7 = (f32[2,128,4]{1,2,0:T(4,128)S(1)}, f32[2,128,4]{1,2,0:T(4,128)}, u32[]{:S(2)}) copy-start(f32[2,128,4]{1,2,0:T(4,128)} %param.13) | copy-start | bytes 12292
  7.2 44.0 %copy-start.5 = (bf16[128,256]{1,0:T(8,128)(2,1)S(1)}, bf16[128,256]{1,0:T(8,128)(2,1)}, u32[]{:S(2)}) copy-start(bf16[128,256]{1,0:T(8,128)(2,1)} %param.16) | copy-start | bytes 196612
  7.2 44.2 %copy-start.4 = (bf16[2,128,256]{2,1,0:T(8,128)(2,1)S(1)}, bf16[2,128,256]{2,1,0:T(8,128)(2,1)}, u32[]{:S(2)}) copy-start(bf16[2,128,256]{2,1,0:T(8,128)(2,1)} %param.15) | copy-start | bytes 393220
  7.2 44.3 %copy-start.6 = (f32[2,128,4]{1,2,0:T(4,128)S(1)}, f32[2,128,4]{1,2,0:T(4,128)}, u32[]{:S(2)}) copy-start(f32[2,128,4]{1,2,0:T(4,128)} %param.14) | copy-start | bytes 12292
  12.5 39.9 %all-to-all-start = ((bf16[8,2,32,128]{3,2,1,0:T(8,128)(2,1)}), bf16[8,2,32,128]{3,2,1,0:T(8,128)(2,1)S(1)}, u32[]{:S(2)}, u32[]{:S(2)}) async-start(bf16[8,2,32,128]{3,2,1,0:T(8,128)(2,1)} %bitcast.20), calls=%async_computation | async-start | bytes 262144 | tf_op jit(solution)/shard_map/all_to_all | solution.py:80
  19.8 107.6 %reduce-scatter.2.cloned.1.call-start = ((), (), s32[]{:S(2)}) async-start(), calls=%async_computation.3 | async-start | bytes 2359296 | tf_op jit(solution)/shard_map/reduce_scatter | solution.py:135
  23.9 30.1 %copy-start.2 = (bf16[4,32,2,2,64]{4,3,2,1,0:T(2,128)(2,1)}, bf16[4,32,2,2,64]{4,3,2,1,0:T(2,128)(2,1)S(1)}, u32[]{:S(2)}) copy-start(bf16[4,32,2,2,64]{4,3,2,1,0:T(2,128)(2,1)S(1)} %reshape_reshape.3) | copy-start | bytes 196612
  54.3 0.9 copy-start.1
  57.3 0.9 copy-start.3
  75.9 13.3 %all-to-all-start.1 = ((bf16[8,2,36,128]{3,1,2,0:T(2,128)(2,1)}), bf16[8,2,36,128]{3,1,2,0:T(2,128)(2,1)S(1)}, u32[]{:S(2)}, u32[]{:S(2)}) async-start(bf16[8,2,36,128]{3,1,2,0:T(2,128)(2,1)} %copy.174), calls=%async_computation.1 | async-start | bytes 294912 | tf_op jit(solution)/shard_map/all_to_all | solution.py:121
Sparse Core Ops, SparseCore 0:
  57.4 69.8 reduce-scatter.1
where the time goes:
time: 137 us; the launch traced here: 136 us
  waiting for transfers between devices  44.6 us (33%)
  blocking collectives  26.6 us (19%)
  other arithmetic  17.5 us (13%)
  local copies, waits for them, and re-layouts  16.2 us (12%)
  between operations  14.5 us (11%)
  starting transfers between devices  11.3 us (8%)
  matrix products  5.35 us (4%)
    reduce_scatter x1, waiting for transfers between devices, shards(): lax.psum_scatter(lax.dot_general(hidden, query_low, (((0,), (0,)), ((), (...  36.1 us
    all_gather x1, blocking collectives, shards(): summaries = lax.all_gather(means, 'kv', axis=0, tiled=True)  26.6 us
    scatter-add x1, other arithmetic, shards(): outgoing = jnp.zeros((blocks_all, groups, BLK, 2 * DH), wide).at[owner, g...  9.74 us
    all_to_all x1, waiting for transfers between devices, shards(): lax.all_to_all(both_out.astype(jnp.bfloat16), 'kv', split_axis=0, concat_...  8.53 us
    all_to_all x1, starting transfers between devices, shards(): lax.all_to_all(outbound, 'kv', split_axis=0, concat_axis=0, tiled=True)  7.31 us
    unnamed x23, local copies, waits for them, and re-layouts  5.95 us
    all_to_all x1, starting transfers between devices, shards(): lax.all_to_all(both_out.astype(jnp.bfloat16), 'kv', split_axis=0, concat_...  3.92 us
    mul x1, other arithmetic, shards(): slot_grads = slot_grads * live[..., None, None].astype(wide)  3.19 us
  transfers between devices with their start and end apart: 3, of which 2 were waited for; matrix products, arithmetic and copies ran while one was open for 20% of the time, Pallas kernels for 0%

commit v1 on v0

--- a/solution.py
+++ b/solution.py
@@ -56,7 +56,9 @@
     means = jnp.mean(pairs.reshape(per_summary, CMP, groups, 2 * DH).astype(wide), 1).astype(
         jnp.bfloat16
     )
-    summaries = lax.all_gather(means, "kv", axis=0, tiled=True)
+    summaries = jnp.concatenate(
+        lax.all_to_all(jnp.stack([means] * lax.axis_size("kv")), "kv", 0, 0), axis=0
+    )
     summary_count = summaries.shape[0]
     sum_keys = jnp.transpose(summaries[..., :DH], (1, 0, 2))
     sum_values = jnp.transpose(summaries[..., DH:], (1, 0, 2))

time: 137 us -> 123 us (0.90)
  blocking collectives: 26.6 us -> 0 us
  waiting for transfers between devices: 44.6 us -> 50.2 us
  starting transfers between devices: 11.3 us -> 16.7 us
    all_gather x1 -> x0, blocking collectives: 26.6 us -> none  [shards(): summaries = lax.all_gather(means, 'kv', axis=0, tiled=True)]
    all_to_all x0 -> x1, starting transfers between devices: none -> 7.31 us  [shards(): lax.all_to_all(jnp.stack([means] * lax.axis_size('kv')), 'kv', 0, 0)]
    all_to_all x1, waiting for transfers between devices: 0.01 us -> 6.93 us  [shards(): lax.all_to_all(outbound, 'kv', split_axis=0, concat_axis=0, tiled=True)]
    unnamed x23 -> x19, local copies, waits for them, and re-layouts: 5.95 us -> 6.85 us
  transfers between devices with their start and end apart: 3 -> 4, of which waited for: 2 -> 3; matrix products, arithmetic and copies ran while one was open for 20% -> 25% of each run, Pallas kernels for 0% -> 0%
where the time goes in v1:
time: 123 us; the launch traced here: 122 us
  waiting for transfers between devices  50.2 us (41%)
  local copies, waits for them, and re-layouts  17.5 us (14%)
  other arithmetic  17.5 us (14%)
  starting transfers between devices  16.7 us (14%)
  between operations  14.5 us (12%)
  matrix products  5.42 us (4%)
    reduce_scatter x1, waiting for transfers between devices, shards(): lax.psum_scatter(lax.dot_general(hidden, query_low, (((0,), (0,)), ((), (...  35.4 us
    scatter-add x1, other arithmetic, shards(): outgoing = jnp.zeros((blocks_all, groups, BLK, 2 * DH), wide).at[owner, g...  9.74 us
    all_to_all x1, waiting for transfers between devices, shards(): lax.all_to_all(both_out.astype(jnp.bfloat16), 'kv', split_axis=0, concat_...  7.89 us
    all_to_all x1, starting transfers between devices, shards(): lax.all_to_all(jnp.stack([means] * lax.axis_size('kv')), 'kv', 0, 0)  7.31 us
    all_to_all x1, waiting for transfers between devices, shards(): lax.all_to_all(outbound, 'kv', split_axis=0, concat_axis=0, tiled=True)  6.93 us
    unnamed x19, local copies, waits for them, and re-layouts  6.85 us
    all_to_all x1, starting transfers between devices, shards(): lax.all_to_all(outbound, 'kv', split_axis=0, concat_axis=0, tiled=True)  5.99 us
    all_to_all x1, starting transfers between devices, shards(): lax.all_to_all(both_out.astype(jnp.bfloat16), 'kv', split_axis=0, concat_...  3.38 us
  transfers between devices with their start and end apart: 4, of which 3 were waited for; matrix products, arithmetic and copies ran while one was open for 25% of the time, Pallas kernels for 0%

profile of v1, /device:TPU:0, one launch (start us, length us, event | category | flops | bytes accessed | tf_op | source)
XLA Modules:
  0.0 121.8 jit_solution(283484282575222371)
XLA Ops:
  7.2 0.9 concatenate.26
  8.1 0.8 concatenate.27
  9.0 0.1 convert_reduce_fusion
  9.1 0.6 stack.2
  9.7 7.3 %all-to-all-start = ((bf16[8,4,2,128]{3,1,2,0:T(4,128)(2,1)}), bf16[8,4,2,128]{3,1,2,0:T(4,128)(2,1)S(1)}, u32[]{:S(2)}, u32[]{:S(2)}) async-start(bf16[8,4,2,128]{3,1,2,0:T(4,128)(2,1)} %stack.2), calls=%async_computation | async-start | bytes 32768 | tf_op jit(solution)/shard_map/all_to_all | solution.py:60
  17.1 0.7 multiply_bitcast_fusion.1
  17.8 0.7 fusion.46
  18.4 0.7 or_select_fusion
  19.1 0.9 fusion.45
  20.1 0.7 fusion.50
  20.8 0.9 fusion.33
  21.7 0.1 copy.193
  21.8 0.1 add.117
  22.0 0.1 reshape.245
  22.1 0.1 add.115
  22.3 1.0 copy.191
  23.2 1.0 copy.192
  24.5 0.1 compare_and_fusion
  24.6 0.1 copy.190
  24.7 0.1 reshape_reshape.3
  24.9 0.1 reshape.261
  25.0 0.1 copy.194
  25.0 0.1 reshape.255
  25.1 0.1 reshape_squeeze.9
  25.2 0.1 reshape_squeeze.11
  25.3 0.1 copy.200
  25.4 1.3 %gather_fusion = bf16[16,32,128]{2,1,0:T(8,128)(2,1)} fusion(bf16[4,32,2,128]{3,1,2,0:T(8,128)(2,1)S(1)} %get-tuple-element.39, s32[16]{0:T(128)S(1)} %reshape.255), kind=kCustom, calls=%fused_computation | custom fusion | bytes 262272 | tf_op jit(solution)/shard_map/gather | solution.py:81
  26.7 6.0 %all-to-all-start.1 = ((bf16[8,2,32,128]{3,2,1,0:T(8,128)(2,1)}), bf16[8,2,32,128]{3,2,1,0:T(8,128)(2,1)S(1)}, u32[]{:S(2)}, u32[]{:S(2)}) async-start(bf16[8,2,32,128]{3,2,1,0:T(8,128)(2,1)} %bitcast.21), calls=%async_computation.1 | async-start | bytes 262144 | tf_op jit(solution)/shard_map/all_to_all | solution.py:82
  32.8 0.1 fusion.18
  32.9 0.2 fusion.19
  33.1 6.9 %all-to-all-done.1 = bf16[8,2,32,128]{3,2,1,0:T(8,128)(2,1)S(1)} async-done(((bf16[8,2,32,128]{3,2,1,0:T(8,128)(2,1)}), bf16[8,2,32,128]{3,2,1,0:T(8,128)(2,1)S(1)}, u32[]{:S(2)}, u32[]{:S(2)}) %all-to-all-start.1) | async-done | bytes 131104 | tf_op jit(solution)/shard_map/all_to_all | solution.py:82
  40.0 1.2 gather_fusion.1
  41.2 0.4 copy.195
  41.6 0.3 fusion.5
  41.9 0.3 fusion.8
  42.2 0.3 fusion.9
  42.5 0.3 copy-done.1
  42.8 0.1 copy.204
  42.9 0.2 fusion.12
  43.1 1.8 %convolution_bitcast_fusion = f32[2048,256]{0,1:T(8,128)} fusion(bf16[128,2048]{1,0:T(8,128)(2,1)S(1)} %copy-done, f32[128,256]{0,1:T(8,128)S(1)} %bitcast.189), kind=kOutput, calls=%fused_computation.3 | convolution fusion | flops 134250496 | bytes 2752512 | tf_op jit(solution)/shard_map/dot_general | solution.py:138
  44.9 0.1 reshape.267
  45.0 0.1 fusion.21
  45.1 0.1 fusion.22
  45.3 0.1 pad_maximum_fusion.2
  45.4 0.4 copy-done.3
  45.8 0.3 fusion.7
  46.1 0.5 copy.206
  46.6 1.4 %convolution_bitcast_fusion.1 = f32[2,4,384,64]{2,3,0,1:T(8,128)S(1)} fusion(f32[4,2,2,32,384]{4,3,2,1,0:T(8,128)} %copy-done.1, bf16[4,32,2,2,64]{4,1,0,3,2:T(8,128)(2,1)S(1)} %bitcast.188), kind=kOutput, calls=%fused_computation.5 | convolution fusion | flops 25362432 | bytes 1638400 | tf_op jit(solution)/shard_map/vmap(grtm,tgre->gme)/dot_general | solution.py:20
  48.0 1.6 %copy.208 = f32[2,4,384,64]{3,2,1,0:T(8,128)} copy(f32[2,4,384,64]{2,3,0,1:T(8,128)S(1)} %convolution_bitcast_fusion.1) | data formatting | bytes 1572864 | tf_op jit(solution)/shard_map/transpose | solution.py:111
  49.7 3.2 %maximum_multiply_fusion = f32[2,48,32,128]{3,2,1,0:T(8,128)} fusion(f32[2,48,32,64]{3,2,1,0:T(8,128)} %bitcast.181, f32[2,48,32,64]{3,2,1,0:T(8,128)S(1)} %bitcast.179, f32[2,48]{1,0:T(2,128)S(1)} %get-tuple-element.34), kind=kLoop, calls=%fused_computation.4 | loop fusion | flops 786432 | bytes 3146112 | tf_op jit(solution)/shard_map/mul | solution.py:113
  52.9 9.7 %scatter_fusion = f32[8,2,32,128]{3,2,1,0:T(8,128)S(1)} fusion(f32[8,2,32,128]{3,2,1,0:T(8,128)S(1)} %broadcast_in_dim.39, s32[96]{0:T(128)S(1)} %reshape.267, f32[96,32,128]{2,1,0:T(8,128)} %bitcast.180), kind=kCustom, calls=%fused_computation.2 | custom fusion | flops 393216 | bytes 4719360 | tf_op jit(solution)/shard_map/scatter-add | solution.py:117
  62.7 0.8 copy.210
  63.5 3.4 %all-to-all-start.2 = ((bf16[8,2,36,128]{3,1,2,0:T(2,128)(2,1)}), bf16[8,2,36,128]{3,1,2,0:T(2,128)(2,1)S(1)}, u32[]{:S(2)}, u32[]{:S(2)}) async-start(bf16[8,2,36,128]{3,1,2,0:T(2,128)(2,1)} %copy.210), calls=%async_computation.2 | async-start | bytes 294912 | tf_op jit(solution)/shard_map/all_to_all | solution.py:123
  66.9 0.1 copy.213
  67.0 0.8 copy.218
  67.7 7.9 %all-to-all-done.2 = bf16[8,2,36,128]{3,1,2,0:T(2,128)(2,1)S(1)} async-done(((bf16[8,2,36,128]{3,1,2,0:T(2,128)(2,1)}), bf16[8,2,36,128]{3,1,2,0:T(2,128)(2,1)S(1)}, u32[]{:S(2)}, u32[]{:S(2)}) %all-to-all-start.2) | async-done | bytes 147488 | tf_op jit(solution)/shard_map/all_to_all | solution.py:123
  75.7 0.1 slice.80
  75.8 0.3 fusion.10
  76.0 0.1 fusion.47
  76.1 0.1 copy.217
  76.2 0.7 copy.220
  77.0 0.7 copy.219
  77.8 35.4 %reduce-scatter.2.cloned.1.call-done = f32[256,256]{0,1:T(8,128)} async-done(((f32[2048,256]{0,1:T(8,128)}), f32[256,256]{0,1:T(8,128)}) %reduce-scatter.2.cloned.1.call-update) | async-done | bytes 262160 | tf_op jit(solution)/shard_map/reduce_scatter | solution.py:137
  113.2 1.8 %copy.221 = f32[256,256]{1,0:T(8,128)} copy(f32[256,256]{0,1:T(8,128)} %reduce-scatter.2.cloned.1.call-done) | data formatting | bytes 524288
  (45 shorter events, 0.7 us)
Async XLA Ops:
  7.2 36.0 %copy-start = (bf16[128,2048]{1,0:T(8,128)(2,1)S(1)}, bf16[128,2048]{1,0:T(8,128)(2,1)}, u32[]{:S(2)}) copy-start(bf16[128,2048]{1,0:T(8,128)(2,1)} %param.12) | copy-start | bytes 1572868
  7.2 17.1 %copy-start.5 = (f32[2,128,4]{1,2,0:T(4,128)S(1)}, f32[2,128,4]{1,2,0:T(4,128)}, u32[]{:S(2)}) copy-start(f32[2,128,4]{1,2,0:T(4,128)} %param.14) | copy-start | bytes 12292
  7.2 17.4 %copy-start.4 = (bf16[128,256]{1,0:T(8,128)(2,1)S(1)}, bf16[128,256]{1,0:T(8,128)(2,1)}, u32[]{:S(2)}) copy-start(bf16[128,256]{1,0:T(8,128)(2,1)} %param.9) | copy-start | bytes 196612
  9.7 17.0 %all-to-all-start = ((bf16[8,4,2,128]{3,1,2,0:T(4,128)(2,1)}), bf16[8,4,2,128]{3,1,2,0:T(4,128)(2,1)S(1)}, u32[]{:S(2)}, u32[]{:S(2)}) async-start(bf16[8,4,2,128]{3,1,2,0:T(4,128)(2,1)} %stack.2), calls=%async_computation | async-start | bytes 32768 | tf_op jit(solution)/shard_map/all_to_all | solution.py:60
  24.9 16.7 %copy-start.2 = (bf16[4,32,2,2,64]{4,3,2,1,0:T(2,128)(2,1)}, bf16[4,32,2,2,64]{4,3,2,1,0:T(2,128)(2,1)S(1)}, u32[]{:S(2)}) copy-start(bf16[4,32,2,2,64]{4,3,2,1,0:T(2,128)(2,1)S(1)} %reshape_reshape.3) | copy-start | bytes 196612
  26.7 13.3 %all-to-all-start.1 = ((bf16[8,2,32,128]{3,2,1,0:T(8,128)(2,1)}), bf16[8,2,32,128]{3,2,1,0:T(8,128)(2,1)S(1)}, u32[]{:S(2)}, u32[]{:S(2)}) async-start(bf16[8,2,32,128]{3,2,1,0:T(8,128)(2,1)} %bitcast.21), calls=%async_computation.1 | async-start | bytes 262144 | tf_op jit(solution)/shard_map/all_to_all | solution.py:82
  32.7 80.5 %reduce-scatter.2.cloned.1.call-start = ((), (), s32[]{:S(2)}) async-start(), calls=%async_computation.4 | async-start | bytes 2359296 | tf_op jit(solution)/shard_map/reduce_scatter | solution.py:137
  41.9 0.9 copy-start.1
  44.9 0.9 copy-start.3
  63.5 12.1 %all-to-all-start.2 = ((bf16[8,2,36,128]{3,1,2,0:T(2,128)(2,1)}), bf16[8,2,36,128]{3,1,2,0:T(2,128)(2,1)S(1)}, u32[]{:S(2)}, u32[]{:S(2)}) async-start(bf16[8,2,36,128]{3,1,2,0:T(2,128)(2,1)} %copy.210), calls=%async_computation.2 | async-start | bytes 294912 | tf_op jit(solution)/shard_map/all_to_all | solution.py:123
Sparse Core Ops, SparseCore 0:
  45.0 68.0 reduce-scatter.1
